TPU v7x, 32 devices: a whole 2x2x4 slice. The times are simulated.
32 devices in a mesh: sp: 8 (over z, x), tp: 4 (over y, core).
Axes of the slice: x: 2, y: 2, z: 4, core: 2. Of those that a mesh axis runs over, the one named last changes fastest.
Arguments:
- tokens: bfloat16 [1024, 2048], P('sp', 'tp'), may hold values from -6 to 6
- conv_value_weight: bfloat16 [2048, 1024], P('sp', 'tp'), may hold values from -0.125 to 0.125
- conv_gate_weight: bfloat16 [2048, 1024], P('sp', 'tp'), may hold values from -0.125 to 0.125
- conv_kernel: bfloat16 [31, 1024], P(None, 'tp'), may hold values from -16 to 16
- conv_norm_gain: float32 [1024], P('tp'), may hold values from 0.1 to 1.9
- query_weight: bfloat16 [2048, 2048], P('sp', 'tp'), may hold values from -0.125 to 0.125
- key_weight: bfloat16 [2048, 2048], P('sp', 'tp'), may hold values from -0.125 to 0.125
- value_weight: bfloat16 [2048, 2048], P('sp', 'tp'), may hold values from -0.125 to 0.125
- input_gate_weight: bfloat16 [2048, 8], P(None, 'tp'), may hold values from -0.125 to 0.125
- forget_gate_weight: bfloat16 [2048, 8], P(None, 'tp'), may hold values from -0.125 to 0.125
- input_offset: float32 [1024, 8], P('sp', 'tp'), may hold values from -4 to 210
- forget_offset: float32 [1024, 8], P('sp', 'tp'), may hold values from 0 to 30
- memory_norm_gain: float32 [2048], P('tp'), may hold values from 0.1 to 1.9
- conv_out_weight: bfloat16 [1024, 2048], P('tp', 'sp'), may hold values from -0.3125 to 0.3125
- memory_out_weight: bfloat16 [2048, 2048], P('tp', 'sp'), may hold values from -0.125 to 0.125
Outputs:
- mixed: bfloat16 [1024, 2048], P('sp', 'tp')
All inputs are finite; a program needn't handle non-finite values.
Results may differ from a plain program's by a relative error of at most 0.03.
Values may be sent and summed in bfloat16 or wider, within the bound.
A program may use at most 128 MiB of HBM per device.

v0:
```python
import jax
import jax.numpy as jnp
from jax import lax
from jax.sharding import PartitionSpec as P

BLOCK = 64
EPS = 1e-06
LOWEST_LEVEL = -1e30


def shifted_2(value, axis, steps):
    count = lax.axis_size(axis)
    leading, last = (max(0, -steps), min(count, count - steps))
    return lax.ppermute(value, axis, [(source, source + steps) for source in range(leading, last)])


def carried_in(shard, axis, join, neutral):
    place = lax.axis_index(axis)
    gathered = jax.tree.map(
        lambda a, kind: lax.all_gather(a.astype(kind), axis),
        shard,
        (jnp.bfloat16, jnp.bfloat16, jnp.bfloat16, jnp.bfloat16),
    )
    state = jax.tree.map(lambda a, e: jnp.zeros_like(a) + jnp.asarray(e, a.dtype), shard, neutral)

    def one(step, state):
        return join(
            state,
            jax.tree.map(
                lambda a, own: lax.dynamic_index_in_dim(a, step, 0, False).astype(own.dtype),
                gathered,
                shard,
            ),
        )

    return lax.fori_loop(0, place, one, state)


def block_step(carry, inputs):
    state, normal, level = carry
    query, key, value, gate_in, forget_log = inputs
    length = gate_in.shape[-1]
    scale = query.shape[-1] ** (-0.5)
    causal = jnp.tril(jnp.ones((length, length), dtype=bool))
    within = jnp.cumsum(forget_log, axis=-1)
    log_weight = within[:, :, None] - within[:, None, :] + gate_in[:, None, :]
    log_weight = jnp.where(causal, log_weight, -jnp.inf)
    carried = within + level[:, None]
    top = jnp.maximum(carried, jnp.max(log_weight, axis=-1))
    weight = jnp.exp(log_weight - top[:, :, None])
    carried_weight = jnp.exp(carried - top) * scale
    scores = jnp.einsum("htd,hsd->hts", query, key, preferred_element_type=jnp.float32) * (
        scale * weight
    )
    numer = jnp.einsum(
        "hts,hse->hte", scores.astype(jnp.bfloat16), value, preferred_element_type=jnp.float32
    )
    numer = numer + carried_weight[:, :, None] * jnp.einsum(
        "hed,htd->hte", state.astype(jnp.bfloat16), query, preferred_element_type=jnp.float32
    )
    denom = jnp.sum(scores, axis=-1) + carried_weight * jnp.einsum(
        "hd,htd->ht", normal.astype(jnp.bfloat16), query, preferred_element_type=jnp.float32
    )
    result = numer / jnp.maximum(jnp.abs(denom), 1.0)[:, :, None]
    last = within[:, -1]
    end_log = last[:, None] - within + gate_in
    new_level = jnp.maximum(last + level, jnp.max(end_log, axis=-1))
    keep = jnp.exp(last + level - new_level)
    fresh = jnp.exp(end_log - new_level[:, None])
    scaled_key = (fresh[:, :, None] * key).astype(jnp.bfloat16)
    new_state = keep[:, None, None] * state + jnp.einsum(
        "hse,hsd->hed", value, scaled_key, preferred_element_type=jnp.float32
    )
    new_normal = keep[:, None] * normal + jnp.sum(scaled_key.astype(jnp.float32), axis=1)
    return ((new_state, new_normal, new_level), result)


def depthwise(extended, kernel):
    taps = kernel.shape[0]
    length = extended.shape[0] - taps + 1
    total = extended[0:length] * kernel[0]
    for index in range(1, taps):
        total = total + extended[index : index + length] * kernel[index]
    return total


def merge_states(first, second):
    first_state, first_normal, first_level, first_total = first
    second_state, second_normal, second_level, second_total = second
    shifted = first_level + second_total
    level = jnp.maximum(shifted, second_level)
    older = jnp.exp(shifted - level)
    newer = jnp.exp(second_level - level)
    state = older[:, None, None] * first_state + newer[:, None, None] * second_state
    normal = older[:, None] * first_normal + newer[:, None] * second_normal
    return (state, normal, level, first_total + second_total)


def on_device(
    tokens,
    conv_value_weight,
    conv_gate_weight,
    conv_kernel,
    conv_norm_gain,
    query_weight,
    key_weight,
    value_weight,
    input_gate_weight,
    forget_gate_weight,
    input_offset,
    forget_offset,
    memory_norm_gain,
    conv_out_weight,
    memory_out_weight,
):
    length = tokens.shape[0]
    heads_here = input_gate_weight.shape[1]
    whole = lax.all_gather(tokens, "tp", axis=1, tiled=True)
    pieces = (
        lax.all_gather(conv_value_weight, "sp", axis=0, tiled=True),
        lax.all_gather(conv_gate_weight, "sp", axis=0, tiled=True),
        lax.all_gather(query_weight, "sp", axis=0, tiled=True),
        lax.all_gather(key_weight, "sp", axis=0, tiled=True),
        lax.all_gather(value_weight, "sp", axis=0, tiled=True),
    )
    folded = tuple((jnp.dot(whole, piece, preferred_element_type=jnp.float32) for piece in pieces))
    conv_value, conv_gate, query_flat, key_flat, value_flat = folded
    gate_pre = jnp.dot(whole, input_gate_weight, preferred_element_type=jnp.float32)
    forget_pre = jnp.dot(whole, forget_gate_weight, preferred_element_type=jnp.float32)
    glu = (conv_value * jax.nn.sigmoid(conv_gate)).astype(jnp.bfloat16)
    taps = conv_kernel.shape[0]
    head_dim = query_flat.shape[1] // heads_here

    def to_heads(flat):
        return flat.astype(jnp.bfloat16).reshape(length, heads_here, head_dim).transpose(1, 0, 2)

    query = to_heads(query_flat)
    key = to_heads(key_flat)
    value = to_heads(value_flat)
    gate_in = (gate_pre + input_offset).T
    forget_log = jax.nn.log_sigmoid(forget_pre + forget_offset).T
    within = jnp.cumsum(forget_log, axis=1)
    total = within[:, -1]
    end_log = total[:, None] - within + gate_in
    local_level = jnp.max(end_log, axis=1)
    fresh = jnp.exp(end_log - local_level[:, None])
    scaled_key = (fresh[:, :, None] * key).astype(jnp.bfloat16)
    local_state = jnp.einsum("hse,hsd->hed", value, scaled_key, preferred_element_type=jnp.float32)
    local_normal = jnp.sum(scaled_key.astype(jnp.float32), axis=1)
    blank_state = (
        jnp.zeros_like(local_state),
        jnp.zeros_like(local_normal),
        jnp.full_like(local_level, LOWEST_LEVEL),
        jnp.zeros_like(total),
    )
    prior = shifted_2(glu[length - (taps - 1) :], "sp", 1)
    incoming = carried_in(
        (local_state, local_normal, local_level, total), "sp", merge_states, blank_state
    )
    extended = jnp.concatenate([prior, glu], axis=0).astype(jnp.float32)
    conv = depthwise(extended, conv_kernel.astype(jnp.float32))
    blocks = length // BLOCK

    def split(array):
        return jnp.moveaxis(array.reshape((heads_here, blocks, BLOCK) + array.shape[2:]), 1, 0)

    _, hidden = lax.scan(
        block_step,
        tuple(incoming[:3]),
        (split(query), split(key), split(value), split(gate_in), split(forget_log)),
    )
    hidden = jnp.moveaxis(hidden, 0, 1).reshape(heads_here, length, head_dim)
    hidden_squares = jnp.sum(hidden * hidden, axis=(0, 2))
    channel_sum, channel_squares, memory_squares = lax.psum(
        (jnp.sum(conv, axis=1), jnp.sum(conv * conv, axis=1), hidden_squares), "tp"
    )
    channels = conv.shape[1] * lax.axis_size("tp")
    mean = (channel_sum / channels)[:, None]
    variance = (channel_squares / channels)[:, None] - mean * mean
    conv_branch = jax.nn.silu((conv - mean) * lax.rsqrt(variance + EPS) * conv_norm_gain).astype(
        jnp.bfloat16
    )
    entries = heads_here * head_dim * lax.axis_size("tp")
    memory_scale = lax.rsqrt(memory_squares / entries + EPS)
    hidden = hidden * memory_scale[None, :, None]
    hidden = hidden * memory_norm_gain.reshape(heads_here, 1, head_dim)
    memory_branch = (
        hidden.transpose(1, 0, 2).reshape(length, heads_here * head_dim).astype(jnp.bfloat16)
    )
    conv_columns, memory_columns = (
        lax.all_gather(conv_out_weight, "sp", axis=1, tiled=True),
        lax.all_gather(memory_out_weight, "sp", axis=1, tiled=True),
    )
    contract = (((0,), (1,)), ((), ()))
    summed = lax.psum_scatter(
        (
            lax.dot_general(conv_columns, conv_branch, contract, preferred_element_type=jnp.float32)
            + lax.dot_general(
                memory_columns, memory_branch, contract, preferred_element_type=jnp.float32
            )
        ).astype(jnp.bfloat16),
        "tp",
        scatter_dimension=0,
        tiled=True,
    ).astype(jnp.float32)
    return summed.T.astype(jnp.bfloat16)


def solution(mesh):
    in_specs = (
        P("sp", "tp"),
        P("sp", "tp"),
        P("sp", "tp"),
        P(None, "tp"),
        P("tp"),
        P("sp", "tp"),
        P("sp", "tp"),
        P("sp", "tp"),
        P(None, "tp"),
        P(None, "tp"),
        P("sp", "tp"),
        P("sp", "tp"),
        P("tp"),
        P("tp", "sp"),
        P("tp", "sp"),
    )
    out_specs = P("sp", "tp")
    return jax.shard_map(
        on_device, mesh=mesh, in_specs=in_specs, out_specs=out_specs, check_vma=False
    )
```

profile of v0, /device:TPU:0, one launch (start us, length us, event | category | flops | bytes accessed | tf_op | source)
XLA Modules:
  0.0 414.2 jit_solution(13057960020475259592)
XLA Ops:
  6.5 0.7 all-gather.22.cloned.1.call-update
  7.3 0.7 all-gather.20.cloned.1.call-update
  8.1 0.7 all-gather.14.cloned.1.call-update
  8.8 0.5 all-gather.16.cloned.1.call-update
  9.4 0.5 all-gather.24.cloned.1.call-update
  10.0 8.9 %all_gather.44 = bf16[128,2048]{1,0:T(8,128)(2,1)S(1)} all-gather(bf16[128,512]{1,0:T(8,128)(2,1)} %param.19), channel_id=1, replica_groups=mesh['sp'=8,'tp'=4] {'tp'}, dimensions={1}, use_global_device_ids=true | all-gather | bytes 655360 | tf_op jit(solution)/shard_map/all_gather | solution.py:118
  18.8 1.0 fusion.87
  19.8 0.3 reduce_window_sum.22
  20.1 0.2 slice_reduce_fusion.1
  20.3 0.4 fusion.94
  20.8 41.0 %all-gather.22.cloned.1.call-done = bf16[2048,512]{1,0:T(8,128)(2,1)} async-done(((bf16[256,512]{1,0:T(8,128)(2,1)}), bf16[2048,512]{1,0:T(8,128)(2,1)}) %all-gather.22.cloned.1.call-update) | async-done | bytes 2097168 | tf_op jit(solution)/shard_map/all_gather | solution.py:123
  61.7 2.0 convolution_convert_fusion.2
  63.8 47.7 %all-gather.20.cloned.1.call-done = bf16[2048,512]{1,0:T(8,128)(2,1)} async-done(((bf16[256,512]{1,0:T(8,128)(2,1)}), bf16[2048,512]{1,0:T(8,128)(2,1)}) %all-gather.20.cloned.1.call-update) | async-done | bytes 2097168 | tf_op jit(solution)/shard_map/all_gather | solution.py:124
  111.5 2.0 convolution_convert_fusion.3
  113.5 1.0 convolution_convert_fusion
  114.7 0.7 all-gather.18.cloned.1.call-update
  115.4 0.7 all-gather.26.cloned.1.call-update
  116.4 0.6 dynamic-slice
  117.7 0.2 dynamic-update-slice.1
  117.9 0.2 dynamic-update-slice
  118.1 34.3 %all-gather.14.cloned.1.call-done = bf16[2048,256]{1,0:T(8,128)(2,1)} async-done(((bf16[256,256]{1,0:T(8,128)(2,1)}), bf16[2048,256]{1,0:T(8,128)(2,1)}) %all-gather.14.cloned.1.call-update) | async-done | bytes 1048592 | tf_op jit(solution)/shard_map/all_gather | solution.py:120
  152.5 1.5 fusion.99
  154.0 39.5 %all-gather.16.cloned.1.call-done = bf16[2048,256]{1,0:T(8,128)(2,1)} async-done(((bf16[256,256]{1,0:T(8,128)(2,1)}), bf16[2048,256]{1,0:T(8,128)(2,1)}) %all-gather.16.cloned.1.call-update) | async-done | bytes 1048592 | tf_op jit(solution)/shard_map/all_gather | solution.py:121
  193.5 1.6 fusion.43
  195.1 2.5 collective-permute-start
  197.6 18.5 %all-reduce.3 = (bf16[16]{0:T(256)(128)(2,1)S(1)}, bf16[16]{0:T(256)(128)(2,1)S(1)}) all-reduce(bf16[16]{0:T(256)(128)(2,1)S(1)} %dynamic-update-slice, bf16[16]{0:T(256)(128)(2,1)S(1)} %dynamic-update-slice.1), channel_id=2, replica_groups=mesh['sp'=8,'tp'=4] {'sp'}, use_global_device_ids=true, to_apply=%add | all-reduce | flops 32 | bytes 128
  216.5 0.6 fusion.90
  217.2 17.5 %all-gather.4 = bf16[8,2,256]{2,1,0:T(2,128)(2,1)S(1)} all-gather(bf16[1,2,256]{2,1,0:T(2,128)(2,1)S(1)} %bitcast.242), channel_id=5, replica_groups=mesh['sp'=8,'tp'=4] {'sp'}, dimensions={0}, use_global_device_ids=true | all-gather | bytes 9216 | tf_op jit(solution)/shard_map/all_gather | solution.py:20
  234.7 8.8 %all-gather.24.cloned.1.call-done = bf16[2048,512]{1,0:T(8,128)(2,1)} async-done(((bf16[256,512]{1,0:T(8,128)(2,1)}), bf16[2048,512]{1,0:T(8,128)(2,1)}) %all-gather.24.cloned.1.call-update) | async-done | bytes 2097168 | tf_op jit(solution)/shard_map/all_gather | solution.py:122
  243.5 2.0 convolution_convert_fusion.1
  245.6 47.6 %all-gather.28.cloned.1.call-done = bf16[16,256,256]{2,1,0:T(8,128)(2,1)} async-done(((bf16[2,256,256]{2,1,0:T(8,128)(2,1)}), bf16[16,256,256]{2,1,0:T(8,128)(2,1)}) %all-gather.28.cloned.1.call-update) | async-done | bytes 2097168 | tf_op jit(solution)/shard_map/all_gather | solution.py:20
  293.3 4.7 %while.33 = (s32[]{:T(128)}, f32[2,256,256]{2,1,0:T(8,128)S(1)}, f32[2,256]{1,0:T(2,128)S(1)}, f32[2]{0:T(128)S(1)}, f32[2,2,64,256]{3,2,0,1:T(8,128)S(1)}, /*in...) while((s32[]{:T(128)}, f32[2,256,256]{2,1,0:T(8,128)S(1)}, ...), condition=%wide.region_15.16_spmd, body=%wide.region_9.15_spmd.sunk | while | flops 42875268 | bytes 2589957 | solution.py:167
  293.3 0.2 reduce_window_sum.24
  293.5 0.2 slice_reduce_fusion.3
  294.3 0.2 fusion.147
  295.0 0.2 fusion.149
  295.2 0.4 convolution_add_fusion.5
  295.6 0.2 reduce_window_sum.24
  295.9 0.2 slice_reduce_fusion.3
  296.6 0.2 fusion.147
  297.3 0.2 fusion.149
  297.6 0.4 convolution_add_fusion.5
  298.2 5.6 %all-reduce.2 = (f32[128]{0:T(128)S(1)}, f32[128]{0:T(128)S(1)}, f32[128]{0:T(128)S(1)}) all-reduce(f32[128]{0:T(128)S(1)} %get-tuple-element.156, f32[128]{0:T(128)S(1)} %get-tuple-element.155, f32[128]{0:T(128)S(1)} %reduce_sum.63), channel_id=1, replica_groups=mesh['sp'=8,'tp'=4] {'tp'}, use_global_device_ids=true, to_apply=%region_3.4 | all-reduce | flops 384 | bytes 3072 | tf_op jit(solution)/shard_map/psum | solution.py:174
  304.1 29.3 %all-gather.18.cloned.1.call-done = bf16[256,2048]{1,0:T(8,128)(2,1)} async-done(((bf16[256,256]{1,0:T(8,128)(2,1)}), bf16[256,2048]{1,0:T(8,128)(2,1)}) %all-gather.18.cloned.1.call-update) | async-done | bytes 1048592 | tf_op jit(solution)/shard_map/all_gather | solution.py:191
  333.4 1.6 fusion.81
  335.0 49.8 %all-gather.26.cloned.1.call-done = bf16[512,2048]{1,0:T(8,128)(2,1)} async-done(((bf16[512,256]{1,0:T(8,128)(2,1)}), bf16[512,2048]{1,0:T(8,128)(2,1)}) %all-gather.26.cloned.1.call-update) | async-done | bytes 2097168 | tf_op jit(solution)/shard_map/all_gather | solution.py:192
  384.8 2.9 fusion.38
  387.7 20.0 %reduce-scatter.2.cloned.1.call-done = bf16[512,128]{0,1:T(8,128)(2,1)} async-done(((bf16[2048,128]{0,1:T(8,128)(2,1)}), bf16[512,128]{0,1:T(8,128)(2,1)}) %reduce-scatter.2.cloned.1.call-update) | async-done | bytes 131088 | tf_op jit(solution)/shard_map/reduce_scatter | solution.py:195
  (81 shorter events, 3.8 us)
Async XLA Ops:
  6.5 13.8 %copy-start = (bf16[2048,2]{0,1:T(2,128)(2,1)S(1)}, bf16[2048,2]{0,1:T(2,128)(2,1)}, u32[]{:S(2)}) copy-start(bf16[2048,2]{0,1:T(2,128)(2,1)} %param.27) | copy-start | bytes 24580
  6.5 13.8 %copy-start.4 = (f32[128,2]{0,1:T(2,128)S(1)}, f32[128,2]{0,1:T(2,128)}, u32[]{:S(2)}) copy-start(f32[128,2]{0,1:T(2,128)} %param.29) | copy-start | bytes 3076
  6.5 55.2 %all-gather.22.cloned.1.call-start = ((), (), s32[]{:S(2)}) async-start(), calls=%async_computation.5 | async-start | bytes 2359296 | tf_op jit(solution)/shard_map/all_gather | solution.py:123
  7.3 104.2 %all-gather.20.cloned.1.call-start = ((), (), s32[]{:S(2)}) async-start(), calls=%async_computation.4 | async-start | bytes 2359296 | tf_op jit(solution)/shard_map/all_gather | solution.py:124
  8.0 144.5 %all-gather.14.cloned.1.call-start = ((), (), s32[]{:S(2)}) async-start(), calls=%async_computation.1 | async-start | bytes 1179648 | tf_op jit(solution)/shard_map/all_gather | solution.py:120
  8.7 184.7 %all-gather.16.cloned.1.call-start = ((), (), s32[]{:S(2)}) async-start(), calls=%async_computation.2 | async-start | bytes 1179648 | tf_op jit(solution)/shard_map/all_gather | solution.py:121
  9.3 234.2 %all-gather.24.cloned.1.call-start = ((), (), s32[]{:S(2)}) async-start(), calls=%async_computation.6 | async-start | bytes 2359296 | tf_op jit(solution)/shard_map/all_gather | solution.py:122
  9.9 283.3 %all-gather.28.cloned.1.call-start = ((), (), s32[]{:S(2)}) async-start(), calls=%async_computation.9 | async-start | bytes 2359296 | tf_op jit(solution)/shard_map/all_gather | solution.py:20
  63.8 52.6 %copy-start.1 = (bf16[31,256]{1,0:T(8,128)(2,1)S(1)}, bf16[31,256]{1,0:T(8,128)(2,1)}, u32[]{:S(2)}) copy-start(bf16[31,256]{1,0:T(8,128)(2,1)} %param.22) | copy-start | bytes 47620
  63.8 52.6 %copy-start.5 = (u32[32]{0:T(128)S(1)}, u32[32]{0:T(128)}, u32[]{:S(2)}) copy-start(u32[32]{0:T(128)} %constant.96) | copy-start | bytes 388
  114.6 101.8 %copy-start.2 = (f32[512]{0:T(512)S(1)}, f32[512]{0:T(512)}, u32[]{:S(2)}) copy-start(f32[512]{0:T(512)} %param.31) | copy-start | bytes 6148
  114.6 218.8 %all-gather.18.cloned.1.call-start = ((), (), s32[]{:S(2)}) async-start(), calls=%async_computation.3 | async-start | bytes 1179648 | tf_op jit(solution)/shard_map/all_gather | solution.py:191
  115.4 269.5 %all-gather.26.cloned.1.call-start = ((), (), s32[]{:S(2)}) async-start(), calls=%async_computation.7 | async-start | bytes 2359296 | tf_op jit(solution)/shard_map/all_gather | solution.py:192
  116.1 291.6 %reduce-scatter.2.cloned.1.call-start = ((), (), s32[]{:S(2)}) async-start(), calls=%async_computation.8 | async-start | bytes 655360 | tf_op jit(solution)/shard_map/reduce_scatter | solution.py:195
  195.1 21.4 %collective-permute-start = (bf16[30,256]{1,0:T(8,128)(2,1)S(1)}, bf16[30,256]{1,0:T(8,128)(2,1)S(1)}, u32[]{:S(2)}, u32[]{:S(2)}) collective-permute-start(bf16[30,256]{1,0:T(8,128)(2,1)S(1)} %slice.259), channel_id=1, source_target_pairs={{0,4},{4,8},{8,12},{12,16},{16,20},{20,24},{24,28},{1,5},{5,9},{9,... | collective-permute-start | bytes 46088 | tf_op jit(solution)/shard_map/ppermute | solution.py:14
  293.3 40.1 %copy-start.3 = (f32[256]{0:T(256)S(1)}, f32[256]{0:T(256)}, u32[]{:S(2)}) copy-start(f32[256]{0:T(256)} %param.23) | copy-start | bytes 3076
Sparse Core Ops, SparseCore 0:
  9.5 52.2 all-gather.21
  63.8 47.6 all-gather.19
  113.6 38.7 all-gather.13
  154.5 38.9 all-gather.15
  195.4 48.0 all-gather.23
  245.5 47.6 all-gather.27
  295.2 38.1 all-gather.17
  335.4 49.3 all-gather.25
  387.8 19.8 reduce-scatter.1
where the time goes:
time: 415 us; the launch traced here: 414 us
  waiting for transfers between devices  323 us (78%)
  blocking collectives  50.5 us (12%)
  matrix products  18.2 us (4%)
  between operations  14.1 us (3%)
    all_gather x1, waiting for transfers between devices, on_device(): lax.all_gather(memory_out_weight, 'sp', axis=1, tiled=True)  49.8 us
    all_gather x1, waiting for transfers between devices, on_device(): lax.all_gather(value_weight, 'sp', axis=0, tiled=True)  47.7 us
    all_gather x1, waiting for transfers between devices, carried_in(): lax.all_gather(a.astype(kind), axis)  47.6 us
    all_gather x1, waiting for transfers between devices, on_device(): lax.all_gather(key_weight, 'sp', axis=0, tiled=True)  41 us
    all_gather x1, waiting for transfers between devices, on_device(): lax.all_gather(conv_gate_weight, 'sp', axis=0, tiled=True)  39.5 us
    all_gather x1, waiting for transfers between devices, on_device(): lax.all_gather(conv_value_weight, 'sp', axis=0, tiled=True)  34.3 us
    all_gather x1, waiting for transfers between devices, on_device(): lax.all_gather(conv_out_weight, 'sp', axis=1, tiled=True)  29.3 us
    reduce_scatter x1, waiting for transfers between devices, on_device(): lax.psum_scatter((lax.dot_general(conv_columns, conv_branch, contract, pr...  20 us
  transfers between devices with their start and end apart: 10, of which 9 were waited for; matrix products, arithmetic and copies ran while one was open for 5% of the time, Pallas kernels for 0%

commit v1 on v0

--- a/solution.py
+++ b/solution.py
@@ -189,7 +189,7 @@
     )
     conv_columns, memory_columns = (
         lax.all_gather(conv_out_weight, "sp", axis=1, tiled=True),
-        lax.all_gather(memory_out_weight, "sp", axis=1, tiled=True),
+        jnp.concatenate(lax.all_gather(memory_out_weight, "sp"), axis=1),
     )
     contract = (((0,), (1,)), ((), ()))
     summed = lax.psum_scatter(

time: 415 us -> 414 us (level)
  no operation moved by 1% of the time
where the time goes in v1:
time: 414 us
  waiting for transfers between devices  320 us (77%)
  blocking collectives  50.5 us (12%)
  matrix products  17 us (4%)
  between operations  14.1 us (3%)
  local copies, waits for them, and re-layouts  5.38 us (1%)
    all_gather x1, waiting for transfers between devices, on_device(): lax.all_gather(value_weight, 'sp', axis=0, tiled=True)  47.7 us
    all_gather x1, waiting for transfers between devices, on_device(): lax.all_gather(memory_out_weight, 'sp')  47.6 us
    all_gather x1, waiting for transfers between devices, carried_in(): lax.all_gather(a.astype(kind), axis)  46.9 us
    all_gather x1, waiting for transfers between devices, on_device(): lax.all_gather(key_weight, 'sp', axis=0, tiled=True)  40 us
    all_gather x1, waiting for transfers between devices, on_device(): lax.all_gather(conv_gate_weight, 'sp', axis=0, tiled=True)  39.5 us
    all_gather x1, waiting for transfers between devices, on_device(): lax.all_gather(conv_value_weight, 'sp', axis=0, tiled=True)  35.2 us
    all_gather x1, waiting for transfers between devices, on_device(): lax.all_gather(conv_out_weight, 'sp', axis=1, tiled=True)  29.3 us
    reduce_scatter x1, waiting for transfers between devices, on_device(): lax.psum_scatter((lax.dot_general(conv_columns, conv_branch, contract, pr...  20.9 us
  transfers between devices with their start and end apart: 10, of which 9 were waited for; matrix products, arithmetic and copies ran while one was open for 5% of the time, Pallas kernels for 0%

profile of v1, /device:TPU:0, one launch (start us, length us, event | category | flops | bytes accessed | tf_op | source)
XLA Modules:
  0.0 413.7 jit_solution(13394603774401688658)
XLA Ops:
  6.5 0.7 all-gather.23.cloned.1.call-update
  7.3 0.7 all-gather.21.cloned.1.call-update
  8.1 0.7 all-gather.15.cloned.1.call-update
  8.8 0.5 all-gather.17.cloned.1.call-update
  9.4 0.5 all-gather.25.cloned.1.call-update
  10.0 0.5 all-gather.29.cloned.1.call-update
  10.5 8.9 %all_gather.47 = bf16[128,2048]{1,0:T(8,128)(2,1)S(1)} all-gather(bf16[128,512]{1,0:T(8,128)(2,1)} %param.19), channel_id=1, replica_groups=mesh['sp'=8,'tp'=4] {'tp'}, dimensions={1}, use_global_device_ids=true | all-gather | bytes 655360 | tf_op jit(solution)/shard_map/all_gather | solution.py:118
  19.4 1.0 fusion.87
  20.4 0.3 reduce_window_sum.22
  20.9 0.4 fusion.94
  21.3 40.0 %all-gather.23.cloned.1.call-done = bf16[2048,512]{1,0:T(8,128)(2,1)} async-done(((bf16[256,512]{1,0:T(8,128)(2,1)}), bf16[2048,512]{1,0:T(8,128)(2,1)}) %all-gather.23.cloned.1.call-update) | async-done | bytes 2097168 | tf_op jit(solution)/shard_map/all_gather | solution.py:123
  61.4 2.0 convolution_convert_fusion.2
  63.4 47.7 %all-gather.21.cloned.1.call-done = bf16[2048,512]{1,0:T(8,128)(2,1)} async-done(((bf16[256,512]{1,0:T(8,128)(2,1)}), bf16[2048,512]{1,0:T(8,128)(2,1)}) %all-gather.21.cloned.1.call-update) | async-done | bytes 2097168 | tf_op jit(solution)/shard_map/all_gather | solution.py:124
  111.1 2.0 convolution_convert_fusion.3
  113.2 1.0 convolution_convert_fusion
  114.3 0.7 all-gather.19.cloned.1.call-update
  115.3 0.6 dynamic-slice
  116.5 0.2 dynamic-update-slice.1
  116.8 0.2 dynamic-update-slice
  117.0 35.2 %all-gather.15.cloned.1.call-done = bf16[2048,256]{1,0:T(8,128)(2,1)} async-done(((bf16[256,256]{1,0:T(8,128)(2,1)}), bf16[2048,256]{1,0:T(8,128)(2,1)}) %all-gather.15.cloned.1.call-update) | async-done | bytes 1048592 | tf_op jit(solution)/shard_map/all_gather | solution.py:120
  152.2 1.5 fusion.99
  153.7 39.5 %all-gather.17.cloned.1.call-done = bf16[2048,256]{1,0:T(8,128)(2,1)} async-done(((bf16[256,256]{1,0:T(8,128)(2,1)}), bf16[2048,256]{1,0:T(8,128)(2,1)}) %all-gather.17.cloned.1.call-update) | async-done | bytes 1048592 | tf_op jit(solution)/shard_map/all_gather | solution.py:121
  193.2 1.6 fusion.43
  194.8 2.5 collective-permute-start
  197.3 18.5 %all-reduce.3 = (bf16[16]{0:T(256)(128)(2,1)S(1)}, bf16[16]{0:T(256)(128)(2,1)S(1)}) all-reduce(bf16[16]{0:T(256)(128)(2,1)S(1)} %dynamic-update-slice, bf16[16]{0:T(256)(128)(2,1)S(1)} %dynamic-update-slice.1), channel_id=2, replica_groups=mesh['sp'=8,'tp'=4] {'sp'}, use_global_device_ids=true, to_apply=%add | all-reduce | flops 32 | bytes 128
  216.2 0.6 fusion.90
  216.9 17.5 %all-gather.5 = bf16[8,2,256]{2,1,0:T(2,128)(2,1)S(1)} all-gather(bf16[1,2,256]{2,1,0:T(2,128)(2,1)S(1)} %bitcast.248), channel_id=5, replica_groups=mesh['sp'=8,'tp'=4] {'sp'}, dimensions={0}, use_global_device_ids=true | all-gather | bytes 9216 | tf_op jit(solution)/shard_map/all_gather | solution.py:20
  234.4 9.0 %all-gather.25.cloned.1.call-done = bf16[2048,512]{1,0:T(8,128)(2,1)} async-done(((bf16[256,512]{1,0:T(8,128)(2,1)}), bf16[2048,512]{1,0:T(8,128)(2,1)}) %all-gather.25.cloned.1.call-update) | async-done | bytes 2097168 | tf_op jit(solution)/shard_map/all_gather | solution.py:122
  243.4 2.0 convolution_convert_fusion.1
  245.5 47.6 %all-gather.29.cloned.1.call-done = bf16[4096,256]{1,0:T(8,128)(2,1)} async-done(((bf16[512,256]{1,0:T(8,128)(2,1)}), bf16[4096,256]{1,0:T(8,128)(2,1)}) %all-gather.29.cloned.1.call-update) | async-done | bytes 2097168 | tf_op jit(solution)/shard_map/all_gather | solution.py:192
  293.0 2.9 copy.58
  295.9 46.9 %all-gather.27.cloned.1.call-done = bf16[16,256,256]{2,1,0:T(8,128)(2,1)} async-done(((bf16[2,256,256]{2,1,0:T(8,128)(2,1)}), bf16[16,256,256]{2,1,0:T(8,128)(2,1)}) %all-gather.27.cloned.1.call-update) | async-done | bytes 2097168 | tf_op jit(solution)/shard_map/all_gather | solution.py:20
  342.9 4.7 %while.33 = (s32[]{:T(128)}, f32[2,256,256]{2,1,0:T(8,128)S(1)}, f32[2,256]{1,0:T(2,128)S(1)}, f32[2]{0:T(128)S(1)}, f32[2,2,64,256]{3,2,0,1:T(8,128)S(1)}, /*in...) while((s32[]{:T(128)}, f32[2,256,256]{2,1,0:T(8,128)S(1)}, ...), condition=%wide.region_15.16_spmd, body=%wide.region_9.15_spmd.sunk | while | flops 42875268 | bytes 2589957 | solution.py:167
  342.9 0.2 reduce_window_sum.24
  343.4 0.2 fusion.144
  343.9 0.2 fusion.147
  344.6 0.2 fusion.149
  344.9 0.4 convolution_add_fusion.5
  345.3 0.2 reduce_window_sum.24
  345.7 0.2 fusion.144
  346.3 0.2 fusion.147
  347.0 0.2 fusion.149
  347.2 0.4 convolution_add_fusion.5
  347.8 5.6 %all-reduce.2 = (f32[128]{0:T(128)S(1)}, f32[128]{0:T(128)S(1)}, f32[128]{0:T(128)S(1)}) all-reduce(f32[128]{0:T(128)S(1)} %get-tuple-element.166, f32[128]{0:T(128)S(1)} %get-tuple-element.165, f32[128]{0:T(128)S(1)} %reduce_sum.63), channel_id=1, replica_groups=mesh['sp'=8,'tp'=4] {'tp'}, use_global_device_ids=true, to_apply=%region_3.4 | all-reduce | flops 384 | bytes 3072 | tf_op jit(solution)/shard_map/psum | solution.py:174
  353.7 29.3 %all-gather.19.cloned.1.call-done = bf16[256,2048]{1,0:T(8,128)(2,1)} async-done(((bf16[256,256]{1,0:T(8,128)(2,1)}), bf16[256,2048]{1,0:T(8,128)(2,1)}) %all-gather.19.cloned.1.call-update) | async-done | bytes 1048592 | tf_op jit(solution)/shard_map/all_gather | solution.py:191
  383.0 1.6 fusion.81
  384.6 1.6 fusion.38
  386.3 20.9 %reduce-scatter.2.cloned.1.call-done = bf16[512,128]{0,1:T(8,128)(2,1)} async-done(((bf16[2048,128]{0,1:T(8,128)(2,1)}), bf16[512,128]{0,1:T(8,128)(2,1)}) %reduce-scatter.2.cloned.1.call-update) | async-done | bytes 131088 | tf_op jit(solution)/shard_map/reduce_scatter | solution.py:195
  (82 shorter events, 4.0 us)
Async XLA Ops:
  6.5 14.3 %copy-start = (bf16[2048,2]{0,1:T(2,128)(2,1)S(1)}, bf16[2048,2]{0,1:T(2,128)(2,1)}, u32[]{:S(2)}) copy-start(bf16[2048,2]{0,1:T(2,128)(2,1)} %param.27) | copy-start | bytes 24580
  6.5 14.4 %copy-start.4 = (f32[128,2]{0,1:T(2,128)S(1)}, f32[128,2]{0,1:T(2,128)}, u32[]{:S(2)}) copy-start(f32[128,2]{0,1:T(2,128)} %param.29) | copy-start | bytes 3076
  6.5 54.8 %all-gather.23.cloned.1.call-start = ((), (), s32[]{:S(2)}) async-start(), calls=%async_computation.5 | async-start | bytes 2359296 | tf_op jit(solution)/shard_map/all_gather | solution.py:123
  7.3 103.9 %all-gather.21.cloned.1.call-start = ((), (), s32[]{:S(2)}) async-start(), calls=%async_computation.4 | async-start | bytes 2359296 | tf_op jit(solution)/shard_map/all_gather | solution.py:124
  8.0 144.2 %all-gather.15.cloned.1.call-start = ((), (), s32[]{:S(2)}) async-start(), calls=%async_computation.1 | async-start | bytes 1179648 | tf_op jit(solution)/shard_map/all_gather | solution.py:120
  8.7 184.4 %all-gather.17.cloned.1.call-start = ((), (), s32[]{:S(2)}) async-start(), calls=%async_computation.2 | async-start | bytes 1179648 | tf_op jit(solution)/shard_map/all_gather | solution.py:121
  9.3 234.1 %all-gather.25.cloned.1.call-start = ((), (), s32[]{:S(2)}) async-start(), calls=%async_computation.6 | async-start | bytes 2359296 | tf_op jit(solution)/shard_map/all_gather | solution.py:122
  9.9 283.1 %all-gather.29.cloned.1.call-start = ((), (), s32[]{:S(2)}) async-start(), calls=%async_computation.9 | async-start | bytes 2359296 | tf_op jit(solution)/shard_map/all_gather | solution.py:192
  10.5 332.3 %all-gather.27.cloned.1.call-start = ((), (), s32[]{:S(2)}) async-start(), calls=%async_computation.8 | async-start | bytes 2359296 | tf_op jit(solution)/shard_map/all_gather | solution.py:20
  63.4 51.8 %copy-start.1 = (bf16[31,256]{1,0:T(8,128)(2,1)S(1)}, bf16[31,256]{1,0:T(8,128)(2,1)}, u32[]{:S(2)}) copy-start(bf16[31,256]{1,0:T(8,128)(2,1)} %param.22) | copy-start | bytes 47620
  63.4 51.9 %copy-start.5 = (u32[32]{0:T(128)S(1)}, u32[32]{0:T(128)}, u32[]{:S(2)}) copy-start(u32[32]{0:T(128)} %constant.96) | copy-start | bytes 388
  114.2 101.9 %copy-start.2 = (f32[512]{0:T(512)S(1)}, f32[512]{0:T(512)}, u32[]{:S(2)}) copy-start(f32[512]{0:T(512)} %param.31) | copy-start | bytes 6148
  114.2 268.8 %all-gather.19.cloned.1.call-start = ((), (), s32[]{:S(2)}) async-start(), calls=%async_computation.3 | async-start | bytes 1179648 | tf_op jit(solution)/shard_map/all_gather | solution.py:191
  115.0 292.2 %reduce-scatter.2.cloned.1.call-start = ((), (), s32[]{:S(2)}) async-start(), calls=%async_computation.7 | async-start | bytes 655360 | tf_op jit(solution)/shard_map/reduce_scatter | solution.py:195
  194.8 21.4 %collective-permute-start = (bf16[30,256]{1,0:T(8,128)(2,1)S(1)}, bf16[30,256]{1,0:T(8,128)(2,1)S(1)}, u32[]{:S(2)}, u32[]{:S(2)}) collective-permute-start(bf16[30,256]{1,0:T(8,128)(2,1)S(1)} %slice.259), channel_id=1, source_target_pairs={{0,4},{4,8},{8,12},{12,16},{16,20},{20,24},{24,28},{1,5},{5,9},{9,... | collective-permute-start | bytes 46088 | tf_op jit(solution)/shard_map/ppermute | solution.py:14
  342.9 40.1 %copy-start.3 = (f32[256]{0:T(256)S(1)}, f32[256]{0:T(256)}, u32[]{:S(2)}) copy-start(f32[256]{0:T(256)} %param.23) | copy-start | bytes 3076
Sparse Core Ops, SparseCore 0:
  9.5 51.8 all-gather.22
  63.5 47.6 all-gather.20
  113.3 38.8 all-gather.14
  154.2 38.9 all-gather.16
  195.1 48.1 all-gather.24
  245.4 47.6 all-gather.28
  295.2 47.6 all-gather.26
  344.9 38.1 all-gather.18
  386.4 20.6 reduce-scatter.1
